TPU v7x, 32 devices: a whole 2x2x4 slice. The times are simulated.
32 devices in a mesh: sp: 16 (over z, y, x), tp: 2 (over core).
Axes of the slice: x: 2, y: 2, z: 4, core: 2. Of those that a mesh axis runs over, the one named last changes fastest.
Arguments:
- resid: bfloat16 [6144, 2048], P('sp'), may hold values from -6 to 6
- x_branch: bfloat16 [6144, 2048], P('sp', 'tp'), may hold values from -6 to 6
- gate_branch: bfloat16 [6144, 2048], P('sp', 'tp'), may hold values from -6 to 6
- conv_w: float32 [4, 2048], P(None, 'tp'), may hold values from -3 to 3
- gate_a_w: bfloat16 [32, 64, 64], P('tp'), may hold values from -0.75 to 0.75
- gate_x_w: bfloat16 [32, 64, 64], P('tp'), may hold values from -0.75 to 0.75
- decay_rate: float32 [2048], P('tp'), may hold values from 0 to 0.01, as said below
- decay_extra: float32 [6144, 2048], P('sp', 'tp'), may hold values from -3 to 0, as said below
- w_proj: bfloat16 [2048, 2048], P('tp'), may hold values from -0.125 to 0.125
- mix_gain: float32 [2048], replicated, may hold values from 0.1 to 1.9
- pre_gain: float32 [2048], replicated, may hold values from 0.1 to 1.9
- w_gate: bfloat16 [2048, 5632], P('sp', 'tp'), may hold values from -0.125 to 0.125
- w_up: bfloat16 [2048, 5632], P('sp', 'tp'), may hold values from -0.125 to 0.125
- w_down: bfloat16 [5632, 2048], P('tp', 'sp'), may hold values from -0.078125 to 0.078125
- out_gain: float32 [2048], replicated, may hold values from 0.1 to 1.9
Outputs:
- stream_out: bfloat16 [6144, 2048], P(('sp', 'tp'))
Inputs may be any that keep to these rules, and one draw needn't show every extreme that they name: `decay_rate`: positive rates. `decay_extra`: non-positive values.
All inputs are finite; a program needn't handle non-finite values.
Results may differ from a plain program's by a relative error of at most 0.015.
Values may be sent and summed in bfloat16 or wider, within the bound.
A program may use at most 128 MiB of HBM per device.

v0:
```python
import jax
import jax.numpy as jnp
from jax import lax
from jax.sharding import PartitionSpec as P

LRU_SCALE = 8.0
NORM_EPS = 1e-06


def from_behind(value, axis, steps):
    count = lax.axis_size(axis)
    first, last = (max(0, -steps), min(count, count - steps))
    return lax.ppermute(value, axis, [(source, source + steps) for source in range(first, last)])


def prefix(part, axis, combine, identity):
    place = lax.axis_index(axis)
    gathered = jax.tree.map(lambda a: lax.all_gather(a, axis), part)
    state = jax.tree.map(lambda a, e: jnp.zeros_like(a) + jnp.asarray(e, a.dtype), part, identity)

    def one(turn, state):
        return combine(
            state, jax.tree.map(lambda a: lax.dynamic_index_in_dim(a, turn, 0, False), gathered)
        )

    return lax.fori_loop(0, place, one, state)


def chain(earlier, later):
    return (earlier[0] * later[0], later[0] * earlier[1] + later[1])


def rms_scale(values, gains):
    return values * lax.rsqrt(jnp.mean(values * values, axis=-1, keepdims=True) + NORM_EPS) * gains


def shards(
    resid,
    x_branch,
    gate_branch,
    conv_w,
    gate_a_w,
    gate_x_w,
    decay_rate,
    decay_extra,
    w_proj,
    mix_gain,
    pre_gain,
    w_gate,
    w_up,
    w_down,
    out_gain,
):
    length = x_branch.shape[0]
    width = x_branch.shape[1]
    taps = conv_w.shape[0]
    before = from_behind(x_branch[length - (taps - 1) :], "sp", 1)
    padded = jnp.concatenate([before, x_branch], axis=0).astype(jnp.float32)
    conv = padded[0:length] * conv_w[0]
    for tap in range(1, taps):
        conv = conv + padded[tap : tap + length] * conv_w[tap]
    conv_out = conv.astype(jnp.bfloat16)
    nblocks = gate_a_w.shape[0]
    grouped = conv_out.reshape(length, nblocks, gate_a_w.shape[1])
    recur = jax.nn.sigmoid(
        jnp.einsum("rnc,ncd->rnd", grouped, gate_a_w, preferred_element_type=jnp.float32).reshape(
            length, width
        )
    )
    inject = jax.nn.sigmoid(
        jnp.einsum("rnc,ncd->rnd", grouped, gate_x_w, preferred_element_type=jnp.float32).reshape(
            length, width
        )
    )
    log_decay = -LRU_SCALE * recur * decay_rate + decay_extra
    decay = jnp.exp(log_decay)
    drive = jnp.sqrt(-jnp.expm1(2.0 * log_decay)) * inject * conv_out.astype(jnp.float32)
    prod_local, state_local = lax.associative_scan(chain, (decay, drive), axis=0)
    identity = (jnp.ones((width,), jnp.float32), jnp.zeros((width,), jnp.float32))
    carried = prefix((prod_local[-1], state_local[-1]), "sp", chain, identity)
    state = state_local + prod_local * carried[1][None, :]
    mixer = (state * jax.nn.gelu(gate_branch.astype(jnp.float32))).astype(jnp.bfloat16)
    share_rows = length // lax.axis_size("tp")
    first = lax.axis_index("tp") * share_rows
    mixed = lax.psum(
        jnp.dot(mixer, w_proj, preferred_element_type=jnp.float32).astype(jnp.bfloat16), "tp"
    ).astype(jnp.float32)
    stream = resid.astype(jnp.float32) + rms_scale(mixed, mix_gain)
    normed = rms_scale(stream, pre_gain).astype(jnp.bfloat16)
    after_mix = lax.dynamic_slice_in_dim(stream, first, share_rows, 0)
    gate_full, up_full = (
        lax.all_gather(w_gate, "sp", axis=0, tiled=True),
        lax.all_gather(w_up, "sp", axis=0, tiled=True),
    )
    down_full = lax.all_gather(w_down, "sp", axis=1, tiled=True)
    gate = jnp.dot(normed, gate_full, preferred_element_type=jnp.float32)
    upward = jnp.dot(normed, up_full, preferred_element_type=jnp.float32)
    hidden = (jax.nn.silu(gate) * upward).astype(jnp.bfloat16)
    ffn = lax.psum_scatter(
        jnp.dot(hidden, down_full, preferred_element_type=jnp.float32).astype(jnp.bfloat16),
        "tp",
        scatter_dimension=0,
        tiled=True,
    ).astype(jnp.float32)
    return (after_mix + 0.5 * rms_scale(ffn, out_gain)).astype(jnp.bfloat16)


def solution(mesh):
    return jax.shard_map(
        shards,
        mesh=mesh,
        in_specs=(
            P("sp", None),
            P("sp", "tp"),
            P("sp", "tp"),
            P(None, "tp"),
            P("tp", None, None),
            P("tp", None, None),
            P("tp"),
            P("sp", "tp"),
            P("tp", None),
            P(),
            P(),
            P("sp", "tp"),
            P("sp", "tp"),
            P("tp", "sp"),
            P(),
        ),
        out_specs=P(("sp", "tp"), None),
        check_vma=False,
    )
```

profile of v0, /device:TPU:0, one launch (start us, length us, event | category | flops | bytes accessed | tf_op | source)
XLA Modules:
  0.0 737.7 jit_solution(13793167642620603508)
XLA Ops:
  8.1 4.9 collective-permute-start
  17.8 1.8 add_divide_fusion.1
  19.6 1.7 copy.106
  21.3 1.8 add_divide_fusion
  23.0 1.6 copy.108
  24.6 5.3 convert_multiply_fusion.7
  30.0 4.5 slice.281
  34.4 2.1 slice.282
  36.6 2.1 slice.280
  38.7 2.2 slice.284
  40.9 3.4 multiply_add_fusion.2
  44.2 2.7 slice.287
  46.9 2.7 slice.288
  49.6 2.7 slice.286
  52.4 2.7 slice.290
  55.1 2.4 multiply_add_fusion.3
  57.4 1.7 slice.293
  59.1 1.7 slice.294
  60.8 1.7 slice.292
  62.5 1.7 slice.296
  64.1 2.0 multiply_add_fusion.4
  67.4 1.6 slice.298
  69.0 1.6 slice.302
  70.6 1.7 multiply_add_fusion.5
  76.6 1.6 multiply_add_fusion.6
  102.2 1.7 slice.291
  103.9 1.7 slice.334
  108.2 2.7 slice.285
  111.0 2.8 slice.336
  116.5 2.3 slice.279
  118.8 2.2 slice.338
  128.0 3.1 pad.113
  135.6 3.2 pad.112
  139.6 42.0 %all-gather.1 = f32[16,1,1024]{2,1,0:T(1,128)S(1)} all-gather(f32[1,1,1024]{2,1,0:T(1,128)S(1)} %add_bitcast_fusion), channel_id=1, replica_groups=mesh['sp'=16,'tp'=2] {'sp'}, dimensions={0}, use_global_device_ids=true | all-gather | bytes 69632 | tf_op jit(solution)/shard_map/all_gather | solution.py:18
  181.7 3.1 pad.129
  184.9 3.2 pad.128
  188.9 35.8 %all-gather = f32[16,1,1024]{2,1,0:T(1,128)S(1)} all-gather(f32[1,1,1024]{2,1,0:T(1,128)S(1)} %add_bitcast_fusion.1), channel_id=1, replica_groups=mesh['sp'=16,'tp'=2] {'sp'}, dimensions={0}, use_global_device_ids=true | all-gather | bytes 69632 | tf_op jit(solution)/shard_map/all_gather | solution.py:18
  224.7 7.0 convolution_convert_fusion.1
  233.6 17.4 %all-reduce.34.cloned.1.call-done = bf16[384,2048]{1,0:T(8,128)(2,1)} async-done(((bf16[384,2048]{1,0:T(8,128)(2,1)}), bf16[384,2048]{1,0:T(8,128)(2,1)}) %all-reduce.34.cloned.1.call-update) | async-done | bytes 1572880 | tf_op jit(solution)/shard_map/psum | solution.py:85
  250.9 1.9 fusion.1
  252.9 2.3 multiply_reduce_fusion
  255.2 119.6 %all-gather.6.cloned.1.call-done = bf16[2048,2816]{1,0:T(8,128)(2,1)} async-done(((bf16[128,2816]{1,0:T(8,128)(2,1)}), bf16[2048,2816]{1,0:T(8,128)(2,1)}) %all-gather.6.cloned.1.call-update) | async-done | bytes 11534352 | tf_op jit(solution)/shard_map/all_gather | solution.py:92
  374.9 9.6 %fusion.43 = f32[384,2816]{1,0:T(8,128)} fusion(bf16[2048,2816]{1,0:T(8,128)(2,1)} %all-gather.6.cloned.1.call-done, f32[384,2048]{1,0:T(8,128)S(1)} %get-tuple-element.61, f32[2048]{0:T(1024)S(1)} %copy-done.38, f32[384]{0:T(512)S(1)} %add_rsqrt_fusion), kind=kOutput, calls=%fused_computation.118 | convolution fusion | flops 4431544320 | bytes 19015168 | tf_op jit(solution)/shard_map/dot_general | solution.py:96
  384.4 173.1 %all-gather.10.cloned.1.call-done = bf16[2816,2048]{1,0:T(8,128)(2,1)} async-done(((bf16[2816,128]{1,0:T(8,128)(2,1)}), bf16[2816,2048]{1,0:T(8,128)(2,1)}) %all-gather.10.cloned.1.call-update) | async-done | bytes 11534352 | tf_op jit(solution)/shard_map/all_gather | solution.py:95
  557.5 142.0 %all-gather.8.cloned.1.call-done = bf16[2048,2816]{1,0:T(8,128)(2,1)} async-done(((bf16[128,2816]{1,0:T(8,128)(2,1)}), bf16[2048,2816]{1,0:T(8,128)(2,1)}) %all-gather.8.cloned.1.call-update) | async-done | bytes 11534352 | tf_op jit(solution)/shard_map/all_gather | solution.py:93
  699.5 19.3 %convolution_convert_fusion = bf16[384,2048]{1,0:T(8,128)(2,1)} fusion(bf16[2816,2048]{1,0:T(8,128)(2,1)} %all-gather.10.cloned.1.call-done, bf16[2048,2816]{1,0:T(8,128)(2,1)} %all-gather.8.cloned.1.call-done, f32[384,2816]{1,0:T(8,128)} %fusion.43, f32[384,2048]{1,0:T(8,128)S(1)} %get-tuple-element.61, f32[2048]{0:T(1024)S(1)} %copy-done.38, ...), kind=kOutput, calls=%fused_computation.12 | convolution fusion | flops 8868003840 | bytes 32122368 | tf_op jit(solution)/shard_map/dot_general | solution.py:100
  718.9 7.4 reduce-scatter.2.cloned.1.call-done
  727.7 2.4 fusion.8
  (205 shorter events, 56.4 us)
Async XLA Ops:
  7.4 10.4 %copy-start = (bf16[16,64,64]{2,1,0:T(8,128)(2,1)S(1)}, bf16[16,64,64]{2,1,0:T(8,128)(2,1)}, u32[]{:S(2)}) copy-start(bf16[16,64,64]{2,1,0:T(8,128)(2,1)} %param.21) | copy-start | bytes 393220
  7.4 243.6 %all-reduce.34.cloned.1.call-start = ((), (), s32[]{:S(2)}) async-start(), calls=%async_computation.1 | async-start | bytes 3145728 | tf_op jit(solution)/shard_map/psum | solution.py:85
  8.1 6.5 collective-permute-start
  19.6 1.7 copy-start.37
  29.9 4.5 copy-start.2
  116.5 5.7 copy-start.15
  116.5 5.7 copy-start.16
  116.5 5.7 copy-start.17
  116.5 6.0 copy-start.18
  116.5 6.0 copy-start.19
  116.5 6.0 copy-start.26
  116.5 6.0 copy-start.27
  118.8 3.8 copy-start.14
  118.8 3.9 copy-start.33
  118.8 3.9 copy-start.32
  121.6 2.1 copy-start.31
  122.2 1.6 copy-start.30
  122.6 1.3 copy-start.13
  122.8 1.2 copy-start.29
  123.7 0.7 copy-start.28
  124.0 0.9 copy-start.11
  124.0 1.0 copy-start.12
  124.5 0.7 copy-start.25
  125.0 0.7 copy-start.24
  125.7 1.0 copy-start.9
  125.7 1.2 copy-start.10
  126.9 0.7 copy-start.23
  128.0 3.1 copy-start.22
  132.5 1.4 copy-start.4
  132.5 1.6 copy-start.5
  134.1 1.4 copy-start.21
  135.6 3.2 copy-start.8
  135.6 46.1 %copy-start.7 = (f32[192,1024]{1,0:T(8,128)S(1)}, f32[192,1024]{1,0:T(8,128)}, u32[]{:S(2)}) copy-start(f32[192,1024]{1,0:T(8,128)} %add.291) | copy-start | bytes 2359300
  138.8 46.0 %copy-start.6 = (f32[191,1024]{1,0:T(8,128)S(1)}, f32[191,1024]{1,0:T(8,128)}, u32[]{:S(2)}) copy-start(f32[191,1024]{1,0:T(8,128)} %get-tuple-element.71) | copy-start | bytes 2347012
  138.8 46.0 %copy-start.20 = (f32[1,1024]{1,0:T(1,128)S(1)}, f32[1,1024]{1,0:T(1,128)}, u32[]{:S(2)}) copy-start(f32[1,1024]{1,0:T(1,128)} %slice.386) | copy-start | bytes 12292
  184.9 39.8 %copy-start.36 = (bf16[384,1024]{1,0:T(8,128)(2,1)S(1)}, bf16[384,1024]{1,0:T(8,128)(2,1)}, u32[]{:S(2)}) copy-start(bf16[384,1024]{1,0:T(8,128)(2,1)} %param.19) | copy-start | bytes 2359300
  231.8 143.1 %all-gather.6.cloned.1.call-start = ((), (), s32[]{:S(2)}) async-start(), calls=%async_computation.2 | async-start | bytes 12255232 | tf_op jit(solution)/shard_map/all_gather | solution.py:92
  232.3 20.5 %copy-start.34 = (f32[2048]{0:T(1024)S(1)}, f32[2048]{0:T(1024)}, u32[]{:S(2)}) copy-start(f32[2048]{0:T(1024)} %param.26) | copy-start | bytes 24580
  232.3 325.2 %all-gather.10.cloned.1.call-start = ((), (), s32[]{:S(2)}) async-start(), calls=%async_computation.4 | async-start | bytes 12255232 | tf_op jit(solution)/shard_map/all_gather | solution.py:95
  232.9 466.6 %all-gather.8.cloned.1.call-start = ((), (), s32[]{:S(2)}) async-start(), calls=%async_computation.3 | async-start | bytes 12255232 | tf_op jit(solution)/shard_map/all_gather | solution.py:93
  233.5 492.8 %reduce-scatter.2.cloned.1.call-start = ((), (), s32[]{:S(2)}) async-start(), calls=%async_computation.5 | async-start | bytes 2359296 | tf_op jit(solution)/shard_map/reduce_scatter | solution.py:99
  250.9 1.9 copy-start.3
  252.9 122.0 %copy-start.38 = (f32[2048]{0:T(1024)S(1)}, f32[2048]{0:T(1024)}, u32[]{:S(2)}) copy-start(f32[2048]{0:T(1024)} %param.27) | copy-start | bytes 24580
  718.9 8.8 %copy-start.35 = (f32[2048]{0:T(1024)S(1)}, f32[2048]{0:T(1024)}, u32[]{:S(2)}) copy-start(f32[2048]{0:T(1024)} %param.31) | copy-start | bytes 24580
  727.7 2.4 copy-start.1
Sparse Core Ops, SparseCore 0:
  231.9 19.0 all-reduce.33
  719.0 7.2 reduce-scatter.1
Sparse Core Ops, SparseCore 1:
  235.0 139.8 all-gather.5
  377.4 180.0 all-gather.9
  560.1 139.3 all-gather.7
where the time goes:
time: 740 us; the launch traced here: 738 us
  waiting for transfers between devices  461 us (62%)
  local copies, waits for them, and re-layouts  103 us (14%)
  blocking collectives  77.8 us (11%)
  matrix products  39.4 us (5%)
  other arithmetic  35.2 us (5%)
  between operations  15.9 us (2%)
    all_gather x1, waiting for transfers between devices, shards(): down_full = lax.all_gather(w_down, 'sp', axis=1, tiled=True)  173 us
    all_gather x1, waiting for transfers between devices, shards(): lax.all_gather(w_up, 'sp', axis=0, tiled=True)  142 us
    all_gather x1, waiting for transfers between devices, shards(): lax.all_gather(w_gate, 'sp', axis=0, tiled=True)  120 us
    slice x56, local copies, waits for them, and re-layouts, shards(): lax.associative_scan(chain, (decay, drive), axis=0)  79.8 us
    all_gather x2, blocking collectives, prefix(): gathered = jax.tree.map(lambda a: lax.all_gather(a, axis), part)  77.8 us
    dot_general x1, matrix products, shards(): jnp.dot(hidden, down_full, preferred_element_type=jnp.float32)  19.3 us
    psum x1, waiting for transfers between devices, shards(): lax.psum(jnp.dot(mixer, w_proj, preferred_element_type=jnp.float32).astyp...  17.4 us
    add x15, other arithmetic, chain(): return (earlier[0] * later[0], later[0] * earlier[1] + later[1])  15 us
  transfers between devices with their start and end apart: 6, of which 5 were waited for; matrix products, arithmetic and copies ran while one was open for 2% of the time, Pallas kernels for 0%

commit v1 on v0

--- a/solution.py
+++ b/solution.py
@@ -92,7 +92,8 @@
         lax.all_gather(w_gate, "sp", axis=0, tiled=True),
         lax.all_gather(w_up, "sp", axis=0, tiled=True),
     )
-    down_full = lax.all_gather(w_down, "sp", axis=1, tiled=True)
+    parts = lax.all_gather(w_down, "sp", axis=0, tiled=False)
+    down_full = jnp.concatenate(parts, axis=1)
     gate = jnp.dot(normed, gate_full, preferred_element_type=jnp.float32)
     upward = jnp.dot(normed, up_full, preferred_element_type=jnp.float32)
     hidden = (jax.nn.silu(gate) * upward).astype(jnp.bfloat16)

time: 740 us -> 702 us (0.949)
  waiting for transfers between devices: 461 us -> 405 us
  local copies, waits for them, and re-layouts: 103 us -> 118 us
    all_gather x1, waiting for transfers between devices: 173 us -> 120 us  [shards(): parts = lax.all_gather(w_down, 'sp', axis=0, tiled=False)]
    reshape x0 -> x1, local copies, waits for them, and re-layouts: none -> 15.2 us  [shards(): down_full = jnp.concatenate(parts, axis=1)]
    all_gather x1, waiting for transfers between devices: 142 us -> 132 us  [shards(): lax.all_gather(w_up, 'sp', axis=0, tiled=True)]
  transfers between devices with their start and end apart: 6 -> 6, of which waited for: 5 -> 5; matrix products, arithmetic and copies ran while one was open for 2% -> 4% of each run, Pallas kernels for 0% -> 0%
where the time goes in v1:
time: 702 us; the launch traced here: 699 us
  waiting for transfers between devices  405 us (58%)
  local copies, waits for them, and re-layouts  118 us (17%)
  blocking collectives  77.8 us (11%)
  matrix products  41.7 us (6%)
  other arithmetic  35.2 us (5%)
  between operations  15.9 us (2%)
    all_gather x1, waiting for transfers between devices, shards(): lax.all_gather(w_up, 'sp', axis=0, tiled=True)  132 us
    all_gather x1, waiting for transfers between devices, shards(): lax.all_gather(w_gate, 'sp', axis=0, tiled=True)  127 us
    all_gather x1, waiting for transfers between devices, shards(): parts = lax.all_gather(w_down, 'sp', axis=0, tiled=False)  120 us
    slice x56, local copies, waits for them, and re-layouts, shards(): lax.associative_scan(chain, (decay, drive), axis=0)  79.8 us
    all_gather x2, blocking collectives, prefix(): gathered = jax.tree.map(lambda a: lax.all_gather(a, axis), part)  77.8 us
    dot_general x1, matrix products, shards(): jnp.dot(hidden, down_full, preferred_element_type=jnp.float32)  21.5 us
    psum x1, waiting for transfers between devices, shards(): lax.psum(jnp.dot(mixer, w_proj, preferred_element_type=jnp.float32).astyp...  17.4 us
    reshape x1, local copies, waits for them, and re-layouts, shards(): down_full = jnp.concatenate(parts, axis=1)  15.2 us
  transfers between devices with their start and end apart: 6, of which 5 were waited for; matrix products, arithmetic and copies ran while one was open for 4% of the time, Pallas kernels for 0%

profile of v1, /device:TPU:0, one launch (start us, length us, event | category | flops | bytes accessed | tf_op | source)
XLA Modules:
  0.0 699.2 jit_solution(6892880732078877363)
XLA Ops:
  8.1 4.9 collective-permute-start
  17.8 1.8 add_divide_fusion.1
  19.6 1.7 copy.110
  21.3 1.8 add_divide_fusion
  23.0 1.6 copy.112
  24.6 5.3 convert_multiply_fusion.7
  30.0 4.5 slice.281
  34.4 2.1 slice.282
  36.6 2.1 slice.280
  38.7 2.2 slice.284
  40.9 3.4 multiply_add_fusion.2
  44.2 2.7 slice.287
  46.9 2.7 slice.288
  49.6 2.7 slice.286
  52.4 2.7 slice.290
  55.1 2.4 multiply_add_fusion.3
  57.4 1.7 slice.293
  59.1 1.7 slice.294
  60.8 1.7 slice.292
  62.5 1.7 slice.296
  64.1 2.0 multiply_add_fusion.4
  67.4 1.6 slice.298
  69.0 1.6 slice.302
  70.6 1.7 multiply_add_fusion.5
  102.2 1.7 slice.291
  103.9 1.7 slice.334
  108.2 2.7 slice.285
  111.0 2.8 slice.336
  116.5 2.3 slice.279
  118.8 2.2 slice.338
  128.0 3.1 pad.113
  135.6 3.2 pad.112
  139.6 42.0 %all-gather.2 = f32[16,1,1024]{2,1,0:T(1,128)S(1)} all-gather(f32[1,1,1024]{2,1,0:T(1,128)S(1)} %add_bitcast_fusion), channel_id=1, replica_groups=mesh['sp'=16,'tp'=2] {'sp'}, dimensions={0}, use_global_device_ids=true | all-gather | bytes 69632 | tf_op jit(solution)/shard_map/all_gather | solution.py:18
  181.7 3.1 pad.129
  184.9 3.2 pad.128
  188.9 35.8 %all-gather.1 = f32[16,1,1024]{2,1,0:T(1,128)S(1)} all-gather(f32[1,1,1024]{2,1,0:T(1,128)S(1)} %add_bitcast_fusion.1), channel_id=1, replica_groups=mesh['sp'=16,'tp'=2] {'sp'}, dimensions={0}, use_global_device_ids=true | all-gather | bytes 69632 | tf_op jit(solution)/shard_map/all_gather | solution.py:18
  224.7 7.0 %convolution_convert_fusion.1 = bf16[384,2048]{1,0:T(8,128)(2,1)} fusion(bf16[1024,2048]{1,0:T(8,128)(2,1)} %param.25, bf16[384,1024]{1,0:T(8,128)(2,1)S(1)} %copy-done.36, f32[384,1024]{1,0:T(8,128)} %pad.128, f32[384,1024]{1,0:T(8,128)} %pad.129, f32[384,1024]{1,0:T(8,128)} %pad.112, f32[384,1024]{1,0:T(8,128)S(1)} %copy-done.8, ...), kind=kOutput, calls=%fused_computation.13 | convolution fusion | flops 1617297408 | bytes 12849152 | tf_op jit(solution)/shard_map/dot_general | solution.py:86
  233.6 17.4 %all-reduce.34.cloned.1.call-done = bf16[384,2048]{1,0:T(8,128)(2,1)} async-done(((bf16[384,2048]{1,0:T(8,128)(2,1)}), bf16[384,2048]{1,0:T(8,128)(2,1)}) %all-reduce.34.cloned.1.call-update) | async-done | bytes 1572880 | tf_op jit(solution)/shard_map/psum | solution.py:85
  250.9 1.9 fusion.1
  252.9 2.3 multiply_reduce_fusion
  255.2 119.6 %all-gather.11.cloned.1.call-done = bf16[45056,128]{1,0:T(8,128)(2,1)} async-done(((bf16[2816,128]{1,0:T(8,128)(2,1)}), bf16[45056,128]{1,0:T(8,128)(2,1)}) %all-gather.11.cloned.1.call-update) | async-done | bytes 11534352 | tf_op jit(solution)/shard_map/all_gather | solution.py:95
  374.9 15.2 %copy.113 = bf16[2816,16,128]{0,2,1:T(8,128)(2,1)} copy(bf16[2816,16,128]{2,0,1:T(8,128)(2,1)} %bitcast.39) | data formatting | bytes 23068672 | tf_op jit(solution)/shard_map/reshape | solution.py:96
  390.1 126.8 %all-gather.7.cloned.1.call-done = bf16[2048,2816]{1,0:T(8,128)(2,1)} async-done(((bf16[128,2816]{1,0:T(8,128)(2,1)}), bf16[2048,2816]{1,0:T(8,128)(2,1)}) %all-gather.7.cloned.1.call-update) | async-done | bytes 11534352 | tf_op jit(solution)/shard_map/all_gather | solution.py:92
  516.9 9.7 %fusion.43 = f32[384,2816]{1,0:T(8,128)} fusion(bf16[2048,2816]{1,0:T(8,128)(2,1)} %all-gather.7.cloned.1.call-done, f32[384,2048]{1,0:T(8,128)S(1)} %get-tuple-element.61, f32[2048]{0:T(1024)S(1)} %copy-done.38, f32[384]{0:T(512)S(1)} %add_rsqrt_fusion), kind=kOutput, calls=%fused_computation.118 | convolution fusion | flops 4431544320 | bytes 19015168 | tf_op jit(solution)/shard_map/dot_general | solution.py:97
  526.6 132.3 %all-gather.9.cloned.1.call-done = bf16[2048,2816]{1,0:T(8,128)(2,1)} async-done(((bf16[128,2816]{1,0:T(8,128)(2,1)}), bf16[2048,2816]{1,0:T(8,128)(2,1)}) %all-gather.9.cloned.1.call-update) | async-done | bytes 11534352 | tf_op jit(solution)/shard_map/all_gather | solution.py:93
  658.9 21.5 %convolution_convert_fusion = bf16[384,2048]{1,0:T(8,128)(2,1)} fusion(bf16[2816,2048]{0,1:T(8,128)(2,1)} %bitcast.40, bf16[2048,2816]{1,0:T(8,128)(2,1)} %all-gather.9.cloned.1.call-done, f32[384,2816]{1,0:T(8,128)} %fusion.43, f32[384,2048]{1,0:T(8,128)S(1)} %get-tuple-element.61, f32[2048]{0:T(1024)S(1)} %copy-done.38, f32[384]{0:T(512)S(1)} %add_rsqrt_fusion), kind=kOutput, calls=%fused_computation.12 | convolution fusion | flops 8868003840 | bytes 32122368 | tf_op jit(solution)/shard_map/dot_general | solution.py:101
  680.4 7.4 %reduce-scatter.2.cloned.1.call-done = bf16[192,2048]{1,0:T(8,128)(2,1)} async-done(((bf16[384,2048]{1,0:T(8,128)(2,1)}), bf16[192,2048]{1,0:T(8,128)(2,1)}) %reduce-scatter.2.cloned.1.call-update) | async-done | bytes 786448 | tf_op jit(solution)/shard_map/reduce_scatter | solution.py:100
  689.2 2.4 fusion.8
  (206 shorter events, 58.0 us)
Async XLA Ops:
  7.4 10.4 %copy-start = (bf16[16,64,64]{2,1,0:T(8,128)(2,1)S(1)}, bf16[16,64,64]{2,1,0:T(8,128)(2,1)}, u32[]{:S(2)}) copy-start(bf16[16,64,64]{2,1,0:T(8,128)(2,1)} %param.21) | copy-start | bytes 393220
  7.4 243.6 %all-reduce.34.cloned.1.call-start = ((), (), s32[]{:S(2)}) async-start(), calls=%async_computation.1 | async-start | bytes 3145728 | tf_op jit(solution)/shard_map/psum | solution.py:85
  8.1 6.5 collective-permute-start
  19.6 1.7 copy-start.37
  29.9 4.5 copy-start.2
  116.5 5.7 copy-start.15
  116.5 5.7 copy-start.16
  116.5 5.7 copy-start.17
  116.5 6.0 copy-start.18
  116.5 6.0 copy-start.19
  116.5 6.0 copy-start.26
  116.5 6.0 copy-start.27
  118.8 3.8 copy-start.14
  118.8 3.9 copy-start.33
  118.8 3.9 copy-start.32
  121.6 2.1 copy-start.31
  122.2 1.6 copy-start.30
  122.6 1.3 copy-start.13
  122.8 1.2 copy-start.29
  123.7 0.7 copy-start.28
  124.0 0.9 copy-start.11
  124.0 1.0 copy-start.12
  124.5 0.7 copy-start.25
  125.0 0.7 copy-start.24
  125.7 1.0 copy-start.9
  125.7 1.2 copy-start.10
  126.9 0.7 copy-start.23
  128.0 3.1 copy-start.22
  132.5 1.4 copy-start.4
  132.5 1.6 copy-start.5
  134.1 1.4 copy-start.21
  135.6 3.2 copy-start.8
  135.6 46.1 %copy-start.7 = (f32[192,1024]{1,0:T(8,128)S(1)}, f32[192,1024]{1,0:T(8,128)}, u32[]{:S(2)}) copy-start(f32[192,1024]{1,0:T(8,128)} %add.291) | copy-start | bytes 2359300
  138.8 46.0 %copy-start.6 = (f32[191,1024]{1,0:T(8,128)S(1)}, f32[191,1024]{1,0:T(8,128)}, u32[]{:S(2)}) copy-start(f32[191,1024]{1,0:T(8,128)} %get-tuple-element.71) | copy-start | bytes 2347012
  138.8 46.0 %copy-start.20 = (f32[1,1024]{1,0:T(1,128)S(1)}, f32[1,1024]{1,0:T(1,128)}, u32[]{:S(2)}) copy-start(f32[1,1024]{1,0:T(1,128)} %slice.386) | copy-start | bytes 12292
  184.9 39.8 %copy-start.36 = (bf16[384,1024]{1,0:T(8,128)(2,1)S(1)}, bf16[384,1024]{1,0:T(8,128)(2,1)}, u32[]{:S(2)}) copy-start(bf16[384,1024]{1,0:T(8,128)(2,1)} %param.19) | copy-start | bytes 2359300
  231.8 143.1 %all-gather.11.cloned.1.call-start = ((), (), s32[]{:S(2)}) async-start(), calls=%async_computation.5 | async-start | bytes 12255232 | tf_op jit(solution)/shard_map/all_gather | solution.py:95
  232.3 20.5 %copy-start.34 = (f32[2048]{0:T(1024)S(1)}, f32[2048]{0:T(1024)}, u32[]{:S(2)}) copy-start(f32[2048]{0:T(1024)} %param.26) | copy-start | bytes 24580
  232.3 284.5 %all-gather.7.cloned.1.call-start = ((), (), s32[]{:S(2)}) async-start(), calls=%async_computation.2 | async-start | bytes 12255232 | tf_op jit(solution)/shard_map/all_gather | solution.py:92
  232.9 426.0 %all-gather.9.cloned.1.call-start = ((), (), s32[]{:S(2)}) async-start(), calls=%async_computation.3 | async-start | bytes 12255232 | tf_op jit(solution)/shard_map/all_gather | solution.py:93
  233.5 454.3 %reduce-scatter.2.cloned.1.call-start = ((), (), s32[]{:S(2)}) async-start(), calls=%async_computation.4 | async-start | bytes 2359296 | tf_op jit(solution)/shard_map/reduce_scatter | solution.py:100
  250.9 1.9 copy-start.3
  374.9 142.0 %copy-start.38 = (f32[2048]{0:T(1024)S(1)}, f32[2048]{0:T(1024)}, u32[]{:S(2)}) copy-start(f32[2048]{0:T(1024)} %param.27) | copy-start | bytes 24580
  680.4 8.8 %copy-start.35 = (f32[2048]{0:T(1024)S(1)}, f32[2048]{0:T(1024)}, u32[]{:S(2)}) copy-start(f32[2048]{0:T(1024)} %param.31) | copy-start | bytes 24580
  689.1 2.4 copy-start.1
Sparse Core Ops, SparseCore 0:
  231.9 19.0 all-reduce.33
  680.5 7.2 reduce-scatter.1
Sparse Core Ops, SparseCore 1:
  235.0 139.8 all-gather.10
  377.5 139.3 all-gather.6
  519.5 139.3 all-gather.8
